TPU v7x, 32 devices: a whole 2x2x4 slice. The times are simulated.
32 devices in a mesh: grp: 2 (over y), sp: 4 (over z), fs: 2 (over x), tp: 2 (over core).
Axes of the slice: x: 2, y: 2, z: 4, core: 2. Of those that a mesh axis runs over, the one named last changes fastest.
Arguments:
- tokens: bfloat16 [4, 512, 2048], P(('grp', 'fs'), 'sp'), parts along dimension 0, may hold values from -6 to 6
- norm_gain: float32 [2048], replicated, may hold values from 0.1 to 1.9
- query_attend: bfloat16 [2048, 8, 128], P(None, ('fs', 'tp')), may hold values from -0.125 to 0.125
- key_attend: bfloat16 [2048, 8, 128], P(None, ('fs', 'tp')), may hold values from -0.125 to 0.125
- value_attend: bfloat16 [2048, 8, 128], P(None, ('fs', 'tp')), may hold values from -0.125 to 0.125
- query_linear: bfloat16 [2048, 8, 128], P(None, ('fs', 'tp')), may hold values from -0.125 to 0.125
- key_linear: bfloat16 [2048, 8, 128], P(None, ('fs', 'tp')), may hold values from -0.125 to 0.125
- value_linear: bfloat16 [2048, 8, 256], P(None, ('fs', 'tp')), may hold values from -0.125 to 0.125
- decay_down: bfloat16 [2048, 32], replicated, may hold values from -0.125 to 0.125
- decay_up: bfloat16 [32, 8, 128], replicated, may hold values from -2.109375 to 2.109375
- decay_bias: float32 [8, 128], replicated, may hold values from -1.5 to 7.5
- log_retain: float32 [4, 512, 8], P(('grp', 'fs'), 'sp'), parts along dimension 0, may hold values from -1.5 to 0
- query_gain: float32 [64], replicated, may hold values from 0.6 to 4
- key_gain: float32 [8, 2, 64], replicated, may hold values from 0.8 to 14
- diff_lambda: float32 [8], replicated, may hold values from 0.3 to 0.8
- mix_gain: float32 [128], replicated, may hold values from 0.1 to 1.9
- state_gain: float32 [256], replicated, may hold values from 0.1 to 1.9
- init_state: float32 [4, 8, 128, 256], P('grp', ('fs', 'tp')), parts along dimension 0, may hold values from -80 to 80
- output_attend: bfloat16 [1024, 2048], P(None, 'tp'), may hold values from -0.109375 to 0.109375
- output_linear: bfloat16 [2048, 2048], P(None, 'tp'), may hold values from -0.109375 to 0.109375
Outputs:
- mixed_out: bfloat16 [4, 512, 2048], P(('grp', 'fs'), 'sp', 'tp'), parts along dimension 0
There are 2 independent parts, one for each index of `grp`. A program takes and returns all parts, laid end to end along the dimension named above; an argument that names none is the same for every part. Nothing has to cross between parts.
All inputs are finite; a program needn't handle non-finite values.
Results may differ from a plain program's by a relative error of at most 0.018.
The roundings to bfloat16 on the way count: a program that leaves them out, or rounds other values in their place, can miss the bound.
Values may be sent and summed in bfloat16 or wider, within the bound.
No kernel may reach another device: no remote copies, remote signals or barrier semaphores. Data moves between devices by JAX's collectives and lax.ppermute only.
A program may use at most 128 MiB of HBM per device.

v0:
```python
import jax
import jax.numpy as jnp
from jax import lax
from jax.sharding import PartitionSpec as P

MIXER_HEADS = 8
HD_A = 64
DV_A = 128
HDK = 128
HDV = 256
BLK = 64
norm_eps = 1e-06
decay_tau = 16.0


def entering(part, axis, combine, identity):
    place = lax.axis_index(axis)
    gathered = jax.tree.map(lambda a: lax.all_gather(a, axis), part)
    state = jax.tree.map(lambda a, e: jnp.zeros_like(a) + jnp.asarray(e, a.dtype), part, identity)

    def one(hop, state):
        return combine(
            state, jax.tree.map(lambda a: lax.dynamic_index_in_dim(a, hop, 0, False), gathered)
        )

    return lax.fori_loop(0, place, one, state)


def rms_scale(values, gain):
    widened = values.astype(jnp.float32)
    return (
        widened * lax.rsqrt(jnp.mean(widened * widened, axis=-1, keepdims=True) + norm_eps) * gain
    )


def head_order(fs_size, tp_size, tp_rank):
    per_device = MIXER_HEADS // (fs_size * tp_size)
    owners = jnp.arange(fs_size, dtype=jnp.int32)[:, None] * tp_size + tp_rank
    return (owners * per_device + jnp.arange(per_device, dtype=jnp.int32)[None, :]).reshape(-1)


def linear_blocks(queries, keys_in, values_in, log_decay):
    tok_rows, head_count, key_dim = queries.shape
    value_dim = values_in.shape[-1]
    block_count = tok_rows // BLK
    highest_precision = lax.Precision.HIGHEST

    def split_blocks(source):
        return source.reshape(block_count, BLK, head_count, source.shape[-1])

    causal = (
        jnp.arange(BLK, dtype=jnp.int32)[:, None] >= jnp.arange(BLK, dtype=jnp.int32)[None, :]
    )[None]

    def advance(carry, inputs_now):
        recurrent_state, offset = carry
        question_patch_lines, block_k, value_tile_width, block_log = inputs_now
        running_state = jnp.cumsum(block_log, axis=0)
        pivot = running_state[BLK // 2]
        q_scaled = question_patch_lines * jnp.exp(running_state - pivot[None])
        k_scaled = block_k * jnp.exp(pivot[None] - running_state)
        scores = jnp.einsum("thk,shk->hts", q_scaled, k_scaled, precision=highest_precision)
        scores = jnp.where(causal, scores, 0.0)
        inside_block = jnp.einsum(
            "hts,shv->thv", scores, value_tile_width, precision=highest_precision
        )
        inside_block = inside_block + jnp.einsum(
            "jwo,wos->jws",
            question_patch_lines * jnp.exp(running_state),
            recurrent_state,
            precision=highest_precision,
        )
        final_state = running_state[-1]
        faded_memory_matrix = block_k * jnp.exp(final_state[None] - running_state)
        recurrent_state = recurrent_state * jnp.exp(final_state)[:, :, None] + jnp.einsum(
            "zcb,zcw->cbw", faded_memory_matrix, value_tile_width, precision=highest_precision
        )
        reaching_keys = question_patch_lines * jnp.exp(offset[None] + running_state)
        return ((recurrent_state, offset + final_state), (inside_block, reaching_keys))

    start_carry = (
        jnp.zeros((head_count, key_dim, value_dim), jnp.float32),
        jnp.zeros((head_count, key_dim), jnp.float32),
    )
    (recurrent_state, total_decay), (inside_block, reaching_keys) = lax.scan(
        advance,
        start_carry,
        (
            split_blocks(queries),
            split_blocks(keys_in),
            split_blocks(values_in),
            split_blocks(log_decay),
        ),
    )
    return (
        recurrent_state,
        total_decay,
        inside_block.reshape(tok_rows, head_count, value_dim),
        reaching_keys.reshape(tok_rows, head_count, key_dim),
    )


def body(
    tokens,
    norm_gain,
    query_attend,
    key_attend,
    value_attend,
    query_linear,
    key_linear,
    value_linear,
    decay_down,
    decay_up,
    decay_bias,
    log_retain,
    query_gain,
    key_gain,
    diff_lambda,
    mix_gain,
    state_gain,
    init_state,
    output_attend,
    output_linear,
):
    fs_size = lax.axis_size("fs")
    tp_size = lax.axis_size("tp")
    tp_rank = lax.axis_index("tp")
    tok_rows = tokens.shape[1]
    normed = rms_scale(tokens, norm_gain).astype(jnp.bfloat16)
    normed_rows = normed[0]
    local_weights = (query_attend, key_attend, value_attend, query_linear, key_linear, value_linear)
    widths = [weight.shape[1] * weight.shape[2] for weight in local_weights]
    packed = jnp.concatenate(
        [weight.reshape(weight.shape[0], -1) for weight in local_weights], axis=1
    )
    computed = jnp.einsum(
        "std,dp->stp",
        lax.all_gather(normed, "fs", axis=0, tiled=True),
        packed,
        preferred_element_type=jnp.float32,
    ).astype(jnp.bfloat16)
    arrived = lax.all_to_all(computed, "fs", split_axis=0, concat_axis=2, tiled=True).reshape(
        tok_rows, fs_size, -1
    )
    sections = []
    column_at = 0
    for weight, width_now in zip(local_weights, widths):
        section = arrived[:, :, column_at : column_at + width_now]
        sections.append(section.reshape(tok_rows, fs_size * weight.shape[1], weight.shape[2]))
        column_at = column_at + width_now
    projected = tuple(sections)
    q_pair, k_pair, v_attend, q_lin, k_lin, v_lin = projected
    head_ids = head_order(fs_size, tp_size, tp_rank)
    head_count = head_ids.shape[0]
    q_unit = rms_scale(q_pair.reshape(tok_rows, head_count, 2, HD_A), query_gain).astype(
        jnp.bfloat16
    )
    k_unit = rms_scale(
        k_pair.reshape(tok_rows, head_count, 2, HD_A), jnp.take(key_gain, head_ids, axis=0)
    ).astype(jnp.bfloat16)
    sp_start = lax.axis_index("sp") * tok_rows
    query_block = (sp_start + jnp.arange(tok_rows, dtype=jnp.int32)) // BLK
    score_scale = HD_A ** (-0.5)
    blank_attend = (
        jnp.full((head_count, 2, tok_rows), -jnp.inf, jnp.float32),
        jnp.zeros((head_count, 2, tok_rows), jnp.float32),
        jnp.zeros((head_count, 2, tok_rows, DV_A), jnp.float32),
    )
    carry = blank_attend
    seg_keys = lax.all_gather(k_unit, "sp", axis=0, tiled=True)
    seg_values = lax.all_gather(v_attend, "sp", axis=0, tiled=True)
    span = seg_keys.shape[0]
    stride_token_lines = 2 * tok_rows
    step_count = span // stride_token_lines
    key_steps = seg_keys.reshape(step_count, stride_token_lines, head_count, 2, HD_A)
    value_steps = seg_values.reshape(step_count, stride_token_lines, head_count, DV_A)

    def one_step(running_state, inputs_now):
        step_index, key_step, value_step = inputs_now
        key_start = step_index * stride_token_lines

        def compute(current):
            run_max, run_total, run_acc = current
            scores = (
                jnp.einsum("qhmd,khmd->hmqk", q_unit, key_step, preferred_element_type=jnp.float32)
                * score_scale
            )
            key_block = (key_start + jnp.arange(stride_token_lines, dtype=jnp.int32)) // BLK
            allowed = query_block[:, None] >= key_block[None, :]
            scores = jnp.where(allowed, scores, -jnp.inf)
            new_max = jnp.maximum(run_max, jnp.max(scores, axis=-1))
            factor = jnp.exp(run_max - new_max)
            raised = jnp.exp(scores - new_max[..., None])
            run_total = run_total * factor + jnp.sum(raised, axis=-1)
            run_acc = run_acc * factor[..., None] + jnp.einsum(
                "hmqk,khv->hmqv",
                raised.astype(jnp.bfloat16),
                value_step,
                preferred_element_type=jnp.float32,
            )
            return (new_max, run_total, run_acc)

        def unchanged(current):
            return current

        return (lax.cond(key_start <= sp_start, compute, unchanged, running_state), None)

    carry, _ = lax.scan(
        one_step, carry, (jnp.arange(step_count, dtype=jnp.int32), key_steps, value_steps)
    )
    run_max, run_total, run_acc = carry
    lambda_heads = jnp.take(diff_lambda, head_ids, axis=0)
    diff_raw = (
        run_acc[:, 0] / run_total[:, 0, :, None]
        - lambda_heads[:, None, None] * run_acc[:, 1] / run_total[:, 1, :, None]
    )
    attend_out = rms_scale(jnp.transpose(diff_raw, (1, 0, 2)), mix_gain).astype(jnp.bfloat16)
    low_rank = jnp.dot(normed_rows, decay_down, preferred_element_type=jnp.float32).astype(
        jnp.bfloat16
    )
    up_columns = jnp.take(decay_up, head_ids, axis=1)
    pre_act = jnp.einsum(
        "tr,rhk->thk", low_rank, up_columns, preferred_element_type=jnp.float32
    ) + jnp.take(decay_bias, head_ids, axis=0)
    retain_heads = jnp.take(log_retain[0], head_ids, axis=1)
    log_decay = jax.nn.log_sigmoid(pre_act) / decay_tau + retain_heads[:, :, None]
    local_state, local_decay, inside_block, reaching_keys = linear_blocks(
        q_lin.astype(jnp.float32) * HDK ** (-0.5),
        k_lin.astype(jnp.float32),
        v_lin.astype(jnp.float32),
        log_decay,
    )

    def chain(earlier, later):
        return (earlier[0] + later[0], earlier[1] * jnp.exp(later[0])[:, :, None] + later[1])

    zero_chain = (jnp.zeros_like(local_decay), jnp.zeros_like(local_state))
    prior_decay, prior_state = entering((local_decay, local_state), "sp", chain, zero_chain)
    start_state = lax.all_to_all(init_state, "fs", split_axis=0, concat_axis=1, tiled=True)[0]
    incoming_state = start_state * jnp.exp(prior_decay)[:, :, None] + prior_state
    linear_raw = inside_block + jnp.einsum(
        "jwo,wos->jws", reaching_keys, incoming_state, precision=lax.Precision.HIGHEST
    )
    linear_out = rms_scale(linear_raw, state_gain).astype(jnp.bfloat16)
    out_cols = output_attend.shape[1]
    per_device = MIXER_HEADS // (fs_size * tp_size)
    attend_view = output_attend.reshape(fs_size, tp_size, per_device * DV_A, out_cols)
    linear_view = output_linear.reshape(fs_size, tp_size, per_device * HDV, out_cols)
    blank_out = jnp.zeros((tok_rows, out_cols), jnp.float32)
    running_out = blank_out
    seg_attend = lax.all_gather(attend_out, "tp", axis=1, tiled=True)
    seg_linear = lax.all_gather(linear_out, "tp", axis=1, tiled=True)
    shard_count = seg_attend.shape[1] // head_count
    first_rank = jnp.int32(0) // head_count
    for shard_step in range(shard_count):
        owner_rank = first_rank + shard_step
        rows_attend = lax.dynamic_index_in_dim(attend_view, owner_rank, 1, keepdims=False).reshape(
            -1, out_cols
        )
        rows_linear = lax.dynamic_index_in_dim(linear_view, owner_rank, 1, keepdims=False).reshape(
            -1, out_cols
        )
        part_attend = seg_attend[
            :, shard_step * head_count : (shard_step + 1) * head_count
        ].reshape(tok_rows, -1)
        part_linear = seg_linear[
            :, shard_step * head_count : (shard_step + 1) * head_count
        ].reshape(tok_rows, -1)
        running_out = running_out + jnp.dot(
            part_attend, rows_attend, preferred_element_type=jnp.float32
        )
        running_out = running_out + jnp.dot(
            part_linear, rows_linear, preferred_element_type=jnp.float32
        )
    return running_out.astype(jnp.bfloat16).reshape(1, tok_rows, out_cols)


def solution(mesh):
    in_specs = (
        P(("grp", "fs"), "sp", None),
        P(),
        P(None, ("fs", "tp"), None),
        P(None, ("fs", "tp"), None),
        P(None, ("fs", "tp"), None),
        P(None, ("fs", "tp"), None),
        P(None, ("fs", "tp"), None),
        P(None, ("fs", "tp"), None),
        P(),
        P(),
        P(),
        P(("grp", "fs"), "sp", None),
        P(),
        P(),
        P(),
        P(),
        P(),
        P("grp", ("fs", "tp"), None, None),
        P(None, "tp"),
        P(None, "tp"),
    )
    out_specs = P(("grp", "fs"), "sp", "tp")
    return jax.shard_map(body, mesh=mesh, in_specs=in_specs, out_specs=out_specs, check_vma=False)
```

profile of v0, /device:TPU:31, one launch (start us, length us, event | category | flops | bytes accessed | tf_op | source)
XLA Modules:
  0.0 174.8 jit_solution(11387450350925184077)
XLA Ops:
  6.6 1.3 fusion.46
  7.9 2.0 %fusion.48 = bf16[1,128,2048]{2,1,0:T(8,128)(2,1)} fusion(bf16[1,128,2048]{2,1,0:T(8,128)(2,1)} %param.28, f32[2048]{0:T(1024)} %param.29, f32[128]{0:T(128)S(1)} %add_rsqrt_fusion.4), kind=kLoop, calls=%fused_computation.92 | loop fusion | flops 1048576 | bytes 1057280 | tf_op jit(solution)/shard_map/convert_element_type | solution.py:129
  10.2 1.3 gather_fusion.1
  11.5 1.3 gather_fusion
  12.8 2.4 %bitcast_dynamic-update-slice_fusion.4 = bf16[2048,1792]{1,0:T(8,128)(2,1)} fusion(bf16[256,8,2,128]{3,2,1,0:T(2,128)(2,1)} %bitcast.243), kind=kLoop, calls=%fused_computation.97 | loop fusion | bytes 2097152
  15.2 2.0 %copy.128 = bf16[256,8,2,256]{3,1,2,0:T(8,128)(2,1)S(1)} copy(bf16[256,8,2,256]{3,2,1,0:T(2,128)(2,1)} %bitcast.240) | data formatting | bytes 4194304
  17.2 0.6 gather_fusion.3
  17.8 0.6 gather_fusion.4
  18.4 0.7 gather_fusion.2
  19.1 2.5 %bitcast_dynamic-update-slice_fusion.3 = bf16[2048,1792]{1,0:T(8,128)(2,1)} fusion(bf16[2048,1792]{1,0:T(8,128)(2,1)} %bitcast_dynamic-update-slice_fusion.4, bf16[256,8,2,128]{3,2,1,0:T(2,128)(2,1)} %bitcast.244), kind=kLoop, calls=%fused_computation.96 | loop fusion | bytes 2097152
  21.6 2.4 %bitcast_dynamic-update-slice_fusion.2 = bf16[2048,1792]{1,0:T(8,128)(2,1)} fusion(bf16[2048,1792]{1,0:T(8,128)(2,1)} %bitcast_dynamic-update-slice_fusion.3, bf16[256,8,2,128]{3,2,1,0:T(2,128)(2,1)} %bitcast.245), kind=kLoop, calls=%fused_computation.95 | loop fusion | bytes 2097152
  24.0 2.5 %bitcast_dynamic-update-slice_fusion.1 = bf16[2048,1792]{1,0:T(8,128)(2,1)} fusion(bf16[2048,1792]{1,0:T(8,128)(2,1)} %bitcast_dynamic-update-slice_fusion.2, bf16[256,8,2,128]{3,2,1,0:T(2,128)(2,1)} %bitcast.246), kind=kLoop, calls=%fused_computation.94 | loop fusion | bytes 2097152
  26.6 1.4 fusion.54
  28.0 2.6 %bitcast_dynamic-update-slice_fusion = bf16[2048,1792]{1,0:T(8,128)(2,1)} fusion(bf16[2048,1792]{1,0:T(8,128)(2,1)} %bitcast_dynamic-update-slice_fusion.1, bf16[256,8,2,128]{3,2,1,0:T(2,128)(2,1)} %bitcast.247), kind=kLoop, calls=%fused_computation.93 | loop fusion | bytes 2097152
  30.6 1.5 constant_dynamic-update-slice_fusion
  32.1 1.6 fusion.68
  33.7 6.4 %fusion.37 = bf16[2,128,1792]{2,1,0:T(8,128)(2,1)} fusion(bf16[2,128,2048]{2,1,0:T(8,128)(2,1)} %all-gather.6.cloned.1.call-done, bf16[2048,1792]{1,0:T(8,128)(2,1)} %constant_dynamic-update-slice_fusion), kind=kOutput, calls=%fused_computation.76 | convolution fusion | flops 1879506944 | bytes 9306112 | tf_op jit(solution)/shard_map/std,dp->stp/dot_general | solution.py:136
  40.1 3.8 %all-to-all-start = ((bf16[2,128,1792]{2,1,0:T(8,128)(2,1)}), bf16[2,128,1792]{2,1,0:T(8,128)(2,1)S(1)}, u32[]{:S(2)}, u32[]{:S(2)}) async-start(bf16[2,128,1792]{2,1,0:T(8,128)(2,1)} %fusion.37), calls=%async_computation | async-start | bytes 1835008 | tf_op jit(solution)/shard_map/all_to_all | solution.py:142
  44.0 4.6 %fusion.67 = (bf16[2,1,512,1024]{3,2,1,0:T(8,128)(2,1)}, bf16[2,1,512,1024]{3,2,1,0:T(8,128)(2,1)}) fusion(bf16[2,2,512,1024]{3,2,1,0:T(8,128)(2,1)} %bitcast.227), kind=kLoop, calls=%fused_computation.147 | loop fusion | bytes 8388608 | tf_op jit(solution)/shard_map/jit(dynamic_index_in_dim)/dynamic_slice | solution.py:260
  48.6 5.8 %all-to-all-done = bf16[2,128,1792]{2,1,0:T(8,128)(2,1)S(1)} async-done(((bf16[2,128,1792]{2,1,0:T(8,128)(2,1)}), bf16[2,128,1792]{2,1,0:T(8,128)(2,1)S(1)}, u32[]{:S(2)}, u32[]{:S(2)}) %all-to-all-start) | async-done | bytes 917536 | tf_op jit(solution)/shard_map/all_to_all | solution.py:142
  54.4 4.7 %all-to-all-start.1 = ((f32[2,2,128,256]{3,2,1,0:T(8,128)}), f32[2,2,128,256]{3,2,1,0:T(8,128)S(1)}, u32[]{:S(2)}, u32[]{:S(2)}) async-start(f32[2,2,128,256]{3,2,1,0:T(8,128)} %param.45), calls=%async_computation.1 | async-start | bytes 1048576 | tf_op jit(solution)/shard_map/all_to_all | solution.py:239
  59.0 0.9 fusion.69
  60.0 1.1 copy.83
  61.6 1.2 copy.94
  62.8 1.6 reshape.336
  64.8 9.1 %while.46 = (s32[]{:T(128)}, f32[4,128,256]{2,1,0:T(8,128)S(1)}, f32[4,128]{1,0:T(4,128)S(1)}, f32[2,64,4,256]{3,1,0,2:T(8,128)}, f32[2,64,4,128]{3,2,1,0:T(4,12...) while((s32[]{:T(128)}, f32[4,128,256]{2,1,0:T(8,128)S(1)}, ...), condition=%wide.region_12.13_spmd.clone, body=%wide.region_10.12_spmd.clone.sunk | while | flops 279794688 | bytes 5934213 | solution.py:85
  64.9 0.9 constant_dynamic-slice_fusion.4
  66.9 1.1 fusion.109
  68.0 0.7 convolution_add_fusion.6
  68.7 0.7 fusion.110
  69.4 0.9 constant_dynamic-slice_fusion.4
  71.4 1.1 fusion.109
  72.6 0.7 convolution_add_fusion.6
  73.3 0.7 fusion.110
  74.0 0.8 copy-done.2
  75.0 13.2 %all_gather.28 = bf16[512,4,2,64]{0,3,2,1:T(8,128)(2,1)S(1)} all-gather(bf16[128,4,2,64]{0,3,2,1:T(8,128)(2,1)S(1)} %multiply_convert_fusion.3), channel_id=1, replica_groups=mesh['grp'=2,'sp'=4,'fs'=2,'tp'=2] {'sp'}, dimensions={0}, use_global_device_ids=true | all-gather | bytes 655360 | tf_op jit(solution)/shard_map/all_gather | solution.py:170
  88.2 1.1 copy.84
  89.4 28.4 %all_gather.29 = bf16[512,4,128]{0,2,1:T(8,128)(2,1)S(1)} all-gather(bf16[128,4,128]{0,2,1:T(8,128)(2,1)S(1)} %bitcast.252), channel_id=1, replica_groups=mesh['grp'=2,'sp'=4,'fs'=2,'tp'=2] {'sp'}, dimensions={0}, use_global_device_ids=true | all-gather | bytes 655360 | tf_op jit(solution)/shard_map/all_gather | solution.py:171
  118.2 0.7 multiply_convert_fusion.2
  119.0 4.9 %while.47 = (s32[]{:T(128)}, f32[4,2,128]{2,1,0:T(2,128)S(1)}, f32[4,2,128]{2,1,0:T(2,128)S(1)}, f32[4,2,128,128]{3,2,1,0:T(8,128)S(1)}, s32[2]{0:T(128)S(1)}, /...) while((s32[]{:T(128)}, f32[4,2,128]{2,1,0:T(2,128)S(1)}, ...), condition=%wide.region_8.9_spmd.clone.clone, body=%wide.region_3.8_spmd.clone.clone.sunk | while | flops 102802176 | bytes 4989555 | solution.py:208
  119.1 0.6 dynamic_slice.111
  120.3 1.2 conditional.4
  121.5 0.6 dynamic_slice.111
  122.8 1.2 conditional.4
  124.5 10.0 %all_gather.30 = bf16[128,8,128]{2,0,1:T(8,128)(2,1)S(1)} all-gather(bf16[128,4,128]{2,0,1:T(8,128)(2,1)S(1)} %multiply_convert_fusion.1), channel_id=1, replica_groups=mesh['grp'=2,'sp'=4,'fs'=2,'tp'=2] {'tp'}, dimensions={1}, use_global_device_ids=true | all-gather | bytes 393216 | tf_op jit(solution)/shard_map/all_gather | solution.py:251
  134.5 0.8 copy.113
  135.3 1.0 copy.101
  136.3 0.8 copy.115
  137.1 8.3 %all-gather.2 = f32[4,4,128]{2,1,0:T(4,128)S(1)} all-gather(f32[1,4,128]{2,1,0:T(4,128)S(1)} %bitcast.260), channel_id=2, replica_groups=mesh['grp'=2,'sp'=4,'fs'=2,'tp'=2] {'sp'}, dimensions={0}, use_global_device_ids=true | all-gather | bytes 10240 | tf_op jit(solution)/shard_map/all_gather | solution.py:18
  145.5 3.9 %while.45 = (s32[]{:T(128)}, f32[4,128]{1,0:T(4,128)S(1)}, f32[4,128,256]{2,1,0:T(8,128)S(1)}, s32[]{:T(128)}, f32[4,4,128]{2,1,0:T(4,128)S(1)}, /*index=5*/f32[...) while((s32[]{:T(128)}, f32[4,128]{1,0:T(4,128)S(1)}, f32[4,128,256]{2,1,0:T(8,128)S(1)}, s32[]{:T(128)}, ...), condition=%wide.region_14.15_spmd, body=%wide.region_13.14_spmd.sunk | while | flops 262661 | bytes 1583239 | solution.py:26
  145.5 1.3 bitcast_add_fusion.4
  146.9 1.2 bitcast_add_fusion.4
  148.2 1.2 bitcast_add_fusion.4
  149.6 2.3 %multiply_reduce_fusion = (f32[128,4]{0,1:T(4,128)S(1)}, f32[128,4,256]{0,2,1:T(8,128)S(1)}) fusion(f32[128,4,256]{0,2,1:T(8,128)} %copy.101, f32[4,128,256]{2,1,0:T(8,128)S(1)} %fusion.49, f32[128,4,128]{2,1,0:T(4,128)} %bitcast.257), kind=kOutput, calls=%fused_computation.104 | convolution fusion | flops 201719296 | bytes 1837056 | tf_op jit(solution)/shard_map/jwo,wos->jws/dot_general | solution.py:241
  151.9 0.8 multiply_convert_fusion
  152.7 1.1 copy.102
  153.8 4.5 %all_gather.35 = bf16[128,8,256]{2,0,1:T(8,128)(2,1)S(1)} all-gather(bf16[128,4,256]{2,0,1:T(8,128)(2,1)S(1)} %copy.102), channel_id=1, replica_groups=mesh['grp'=2,'sp'=4,'fs'=2,'tp'=2] {'tp'}, dimensions={1}, use_global_device_ids=true | all-gather | bytes 786432 | tf_op jit(solution)/shard_map/all_gather | solution.py:252
  158.3 0.7 fusion.70
  159.0 1.8 %copy.114 = bf16[128,4,256]{0,2,1:T(8,128)(2,1)} copy(bf16[128,4,256]{2,0,1:T(8,128)(2,1)} %get-tuple-element.513) | data formatting | bytes 524288
  160.8 0.8 copy.116
  161.6 2.2 %fusion.73 = f32[128,1024]{1,0:T(8,128)S(1)} fusion(bf16[128,1024]{0,1:T(8,128)(2,1)} %bitcast.249, bf16[1024,1024]{1,0:T(8,128)(2,1)} %bitcast.225), kind=kOutput, calls=%fused_computation.153 | convolution fusion | flops 268435456 | bytes 2883584 | tf_op jit(solution)/shard_map/dot_general | solution.py:272
  163.8 1.4 fusion.74
  165.3 1.6 convolution_add_fusion.3
  166.9 1.0 fusion.43
  (121 shorter events, 7.5 us)
Async XLA Ops:
  6.5 20.1 %copy-start = (bf16[2048,32]{0,1:T(8,128)(2,1)S(1)}, bf16[2048,32]{0,1:T(8,128)(2,1)}, u32[]{:S(2)}) copy-start(bf16[2048,32]{0,1:T(8,128)(2,1)} %param.36) | copy-start | bytes 393220
  6.5 10.7 %copy-start.10 = (f32[8,128]{1,0:T(8,128)S(1)}, f32[8,128]{1,0:T(8,128)}, u32[]{:S(2)}) copy-start(f32[8,128]{1,0:T(8,128)} %param.38) | copy-start | bytes 12292
  6.5 11.2 %copy-start.1 = (f32[1,128,8]{1,2,0:T(8,128)S(1)}, f32[1,128,8]{1,2,0:T(8,128)}, u32[]{:S(2)}) copy-start(f32[1,128,8]{1,2,0:T(8,128)} %param.39) | copy-start | bytes 12292
  6.5 11.8 %copy-start.7 = (bf16[32,8,128]{2,1,0:T(8,128)(2,1)S(1)}, bf16[32,8,128]{2,1,0:T(8,128)(2,1)}, u32[]{:S(2)}) copy-start(bf16[32,8,128]{2,1,0:T(8,128)(2,1)} %param.37) | copy-start | bytes 196612
  6.5 27.1 %all-gather.6.cloned.1.call-start = ((), (), s32[]{:S(2)}) async-start(), calls=%async_computation.2 | async-start | bytes 1572864 | tf_op jit(solution)/shard_map/all_gather | solution.py:138
  9.9 16.7 %copy-start.6 = (bf16[1,128,2048]{2,1,0:T(8,128)(2,1)S(1)}, bf16[1,128,2048]{2,1,0:T(8,128)(2,1)}, u32[]{:S(2)}) copy-start(bf16[1,128,2048]{2,1,0:T(8,128)(2,1)} %fusion.48) | copy-start | bytes 1572868
  28.0 4.1 %copy-start.5 = (bf16[1024,1024]{1,0:T(8,128)(2,1)S(1)}, bf16[1024,1024]{1,0:T(8,128)(2,1)}, u32[]{:S(2)}) copy-start(bf16[1024,1024]{1,0:T(8,128)(2,1)} %param.46) | copy-start | bytes 6291460
  40.1 14.3 %all-to-all-start = ((bf16[2,128,1792]{2,1,0:T(8,128)(2,1)}), bf16[2,128,1792]{2,1,0:T(8,128)(2,1)S(1)}, u32[]{:S(2)}, u32[]{:S(2)}) async-start(bf16[2,128,1792]{2,1,0:T(8,128)(2,1)} %fusion.37), calls=%async_computation | async-start | bytes 1835008 | tf_op jit(solution)/shard_map/all_to_all | solution.py:142
  54.4 95.0 %all-to-all-start.1 = ((f32[2,2,128,256]{3,2,1,0:T(8,128)}), f32[2,2,128,256]{3,2,1,0:T(8,128)S(1)}, u32[]{:S(2)}, u32[]{:S(2)}) async-start(f32[2,2,128,256]{3,2,1,0:T(8,128)} %param.45), calls=%async_computation.1 | async-start | bytes 1048576 | tf_op jit(solution)/shard_map/all_to_all | solution.py:239
  59.0 86.4 %all-gather.8.cloned.1.call-start = ((), (), s32[]{:S(2)}) async-start(), calls=%async_computation.3 | async-start | bytes 2621440 | tf_op jit(solution)/shard_map/all_gather | solution.py:18
  74.0 0.8 copy-start.2
  119.0 5.3 %copy-start.12 = (f32[128]{0:T(128)S(1)}, f32[128]{0:T(128)}, u32[]{:S(2)}) copy-start(f32[128]{0:T(128)} %param.43) | copy-start | bytes 1540
  119.0 16.3 %copy-start.9 = (f32[2,64,4,256]{3,1,0,2:T(8,128)S(1)}, f32[2,64,4,256]{3,1,0,2:T(8,128)}, u32[]{:S(2)}) copy-start(f32[2,64,4,256]{3,1,0,2:T(8,128)} %get-tuple-element.232) | copy-start | bytes 1572868
  124.5 27.4 %copy-start.11 = (f32[256]{0:T(256)S(1)}, f32[256]{0:T(256)}, u32[]{:S(2)}) copy-start(f32[256]{0:T(256)} %param.44) | copy-start | bytes 3076
  145.5 18.4 %copy-start.3 = (bf16[2,1,512,1024]{3,2,1,0:T(8,128)(2,1)S(1)}, bf16[2,1,512,1024]{3,2,1,0:T(8,128)(2,1)}, u32[]{:S(2)}) copy-start(bf16[2,1,512,1024]{3,2,1,0:T(8,128)(2,1)} %get-tuple-element.506) | copy-start | bytes 6291460
  149.6 17.4 %copy-start.4 = (bf16[2,1,256,1024]{3,2,1,0:T(8,128)(2,1)S(1)}, bf16[2,1,256,1024]{3,2,1,0:T(8,128)(2,1)}, u32[]{:S(2)}) copy-start(bf16[2,1,256,1024]{3,2,1,0:T(8,128)(2,1)} %get-tuple-element.507) | copy-start | bytes 3145732
  161.6 5.3 %copy-start.8 = (bf16[128,4,128]{0,2,1:T(8,128)(2,1)S(1)}, bf16[128,4,128]{0,2,1:T(8,128)(2,1)}, u32[]{:S(2)}) copy-start(bf16[128,4,128]{0,2,1:T(8,128)(2,1)} %copy.115) | copy-start | bytes 393220
Sparse Core Ops, SparseCore 0:
  10.1 21.0 all-gather.5
  74.9 55.7 all-gather.7
where the time goes:
time: 176 us; the launch traced here: 175 us
  blocking collectives  64.4 us (37%)
  local copies, waits for them, and re-layouts  44 us (25%)
  matrix products  23.2 us (13%)
  between operations  13.8 us (8%)
  other arithmetic  13.4 us (8%)
  starting transfers between devices  8.49 us (5%)
  waiting for transfers between devices  5.8 us (3%)
    all_gather x1, blocking collectives, body(): seg_values = lax.all_gather(v_attend, 'sp', axis=0, tiled=True)  28.4 us
    unnamed x37, local copies, waits for them, and re-layouts  19.5 us
    all_gather x1, blocking collectives, body(): seg_keys = lax.all_gather(k_unit, 'sp', axis=0, tiled=True)  13.2 us
    all_gather x1, blocking collectives, body(): seg_attend = lax.all_gather(attend_out, 'tp', axis=1, tiled=True)  10 us
    all_gather x1, blocking collectives, entering(): gathered = jax.tree.map(lambda a: lax.all_gather(a, axis), part)  8.34 us
    dot_general x1, matrix products, body(): jnp.einsum('std,dp->stp', lax.all_gather(normed, 'fs', axis=0, tiled=True...  6.43 us
    all_to_all x1, waiting for transfers between devices, body(): lax.all_to_all(computed, 'fs', split_axis=0, concat_axis=2, tiled=True)  5.76 us
    all_to_all x1, starting transfers between devices, body(): lax.all_to_all(init_state, 'fs', split_axis=0, concat_axis=1, tiled=True)[0]  4.65 us
  transfers between devices with their start and end apart: 4, of which 1 were waited for; matrix products, arithmetic and copies ran while one was open for 32% of the time, Pallas kernels for 0%

commit v1 on v0

--- a/solution.py
+++ b/solution.py
@@ -168,7 +168,12 @@
     )
     carry = blank_attend
     seg_keys = lax.all_gather(k_unit, "sp", axis=0, tiled=True)
-    seg_values = lax.all_gather(v_attend, "sp", axis=0, tiled=True)
+    ring = [v_attend]
+    for hop_ in range(3):
+        ring.append(lax.ppermute(ring[-1], "sp", [(dev, (dev + 1) % 4) for dev in range(4)]))
+    seg_values = jnp.roll(
+        jnp.concatenate(ring[::-1], axis=0), (lax.axis_index("sp") + 1) * ring[0].shape[0], axis=0
+    )
     span = seg_keys.shape[0]
     stride_token_lines = 2 * tok_rows
     step_count = span // stride_token_lines

time: 176 us -> 167 us (0.949)
  blocking collectives: 64.4 us -> 33.9 us
  waiting for transfers between devices: 5.8 us -> 20.5 us
  starting transfers between devices: 8.49 us -> 15.6 us
    all_gather x1 -> x0, blocking collectives: 28.4 us -> none  [body(): seg_values = lax.all_gather(v_attend, 'sp', axis=0, tiled=True)]
    ppermute x0 -> x3, waiting for transfers between devices: none -> 12.8 us  [body(): lax.ppermute(ring[-1], 'sp', [(dev, (dev + 1) % 4) for dev in range(4)])]
    ppermute x0 -> x3, starting transfers between devices: none -> 7.15 us  [body(): lax.ppermute(ring[-1], 'sp', [(dev, (dev + 1) % 4) for dev in range(4)])]
    all_gather x1, blocking collectives: 4.48 us -> 2.32 us  [body(): seg_linear = lax.all_gather(linear_out, 'tp', axis=1, tiled=True)]
    all_gather x1, waiting for transfers between devices: 0.01 us -> 2.02 us  [entering(): gathered = jax.tree.map(lambda a: lax.all_gather(a, axis), part)]
    convert_element_type x2, local copies, waits for them, and re-layouts: 2.76 us -> 0.92 us  [body(): v_lin.astype(jnp.float32)]
    unnamed x37 -> x46, local copies, waits for them, and re-layouts: 19.5 us -> 20.7 us
  transfers between devices with their start and end apart: 4 -> 7, of which waited for: 1 -> 4; matrix products, arithmetic and copies ran while one was open for 32% -> 34% of each run, Pallas kernels for 0% -> 0%
where the time goes in v1:
time: 167 us; the launch traced here: 166 us
  local copies, waits for them, and re-layouts  43.2 us (26%)
  blocking collectives  33.9 us (20%)
  matrix products  23.2 us (14%)
  waiting for transfers between devices  20.5 us (12%)
  starting transfers between devices  15.6 us (9%)
  between operations  13.9 us (8%)
  other arithmetic  13.4 us (8%)
  loops' own time  1.67 us (1%)
    unnamed x46, local copies, waits for them, and re-layouts  20.7 us
    ppermute x3, waiting for transfers between devices, body(): lax.ppermute(ring[-1], 'sp', [(dev, (dev + 1) % 4) for dev in range(4)])  12.8 us
    all_gather x1, blocking collectives, body(): seg_keys = lax.all_gather(k_unit, 'sp', axis=0, tiled=True)  12 us
    all_gather x1, blocking collectives, body(): seg_attend = lax.all_gather(attend_out, 'tp', axis=1, tiled=True)  10.8 us
    all_gather x1, blocking collectives, entering(): gathered = jax.tree.map(lambda a: lax.all_gather(a, axis), part)  8.74 us
    ppermute x3, starting transfers between devices, body(): lax.ppermute(ring[-1], 'sp', [(dev, (dev + 1) % 4) for dev in range(4)])  7.15 us
    dot_general x1, matrix products, body(): jnp.einsum('std,dp->stp', lax.all_gather(normed, 'fs', axis=0, tiled=True...  6.41 us
    all_to_all x1, waiting for transfers between devices, body(): lax.all_to_all(computed, 'fs', split_axis=0, concat_axis=2, tiled=True)  5.69 us
  transfers between devices with their start and end apart: 7, of which 4 were waited for; matrix products, arithmetic and copies ran while one was open for 34% of the time, Pallas kernels for 0%

profile of v1, /device:TPU:31, one launch (start us, length us, event | category | flops | bytes accessed | tf_op | source)
XLA Modules:
  0.0 165.5 jit_solution(12980924709978730441)
XLA Ops:
  6.6 1.3 fusion.46
  7.9 2.1 %fusion.48 = bf16[1,128,2048]{2,1,0:T(8,128)(2,1)} fusion(bf16[1,128,2048]{2,1,0:T(8,128)(2,1)} %param.28, f32[2048]{0:T(1024)} %param.29, f32[128]{0:T(128)S(1)} %add_rsqrt_fusion.4), kind=kLoop, calls=%fused_computation.92 | loop fusion | flops 1048576 | bytes 1057280 | tf_op jit(solution)/shard_map/convert_element_type | solution.py:129
  10.2 2.4 %bitcast_dynamic-update-slice_fusion.4 = bf16[2048,1792]{1,0:T(8,128)(2,1)} fusion(bf16[256,8,2,128]{3,2,1,0:T(2,128)(2,1)} %bitcast.246), kind=kLoop, calls=%fused_computation.97 | loop fusion | bytes 2097152
  12.7 2.0 %copy.128 = bf16[256,8,2,256]{3,1,2,0:T(8,128)(2,1)S(1)} copy(bf16[256,8,2,256]{3,2,1,0:T(2,128)(2,1)} %bitcast.240) | data formatting | bytes 4194304
  14.7 0.6 gather_fusion.1
  17.1 0.7 gather_fusion.2
  17.8 2.5 %bitcast_dynamic-update-slice_fusion.3 = bf16[2048,1792]{1,0:T(8,128)(2,1)} fusion(bf16[2048,1792]{1,0:T(8,128)(2,1)} %bitcast_dynamic-update-slice_fusion.4, bf16[256,8,2,128]{3,2,1,0:T(2,128)(2,1)} %bitcast.247), kind=kLoop, calls=%fused_computation.96 | loop fusion | bytes 2097152
  20.3 2.4 %bitcast_dynamic-update-slice_fusion.2 = bf16[2048,1792]{1,0:T(8,128)(2,1)} fusion(bf16[2048,1792]{1,0:T(8,128)(2,1)} %bitcast_dynamic-update-slice_fusion.3, bf16[256,8,2,128]{3,2,1,0:T(2,128)(2,1)} %bitcast.248), kind=kLoop, calls=%fused_computation.95 | loop fusion | bytes 2097152
  22.8 2.4 %bitcast_dynamic-update-slice_fusion.1 = bf16[2048,1792]{1,0:T(8,128)(2,1)} fusion(bf16[2048,1792]{1,0:T(8,128)(2,1)} %bitcast_dynamic-update-slice_fusion.2, bf16[256,8,2,128]{3,2,1,0:T(2,128)(2,1)} %bitcast.249), kind=kLoop, calls=%fused_computation.94 | loop fusion | bytes 2097152
  25.3 1.4 fusion.54
  26.7 2.5 %bitcast_dynamic-update-slice_fusion = bf16[2048,1792]{1,0:T(8,128)(2,1)} fusion(bf16[2048,1792]{1,0:T(8,128)(2,1)} %bitcast_dynamic-update-slice_fusion.1, bf16[256,8,2,128]{3,2,1,0:T(2,128)(2,1)} %bitcast.250), kind=kLoop, calls=%fused_computation.93 | loop fusion | bytes 2097152
  29.2 1.5 constant_dynamic-update-slice_fusion
  30.8 1.6 fusion.68
  32.4 6.4 %fusion.37 = bf16[2,128,1792]{2,1,0:T(8,128)(2,1)} fusion(bf16[2,128,2048]{2,1,0:T(8,128)(2,1)} %all-gather.6.cloned.1.call-done, bf16[2048,1792]{1,0:T(8,128)(2,1)} %constant_dynamic-update-slice_fusion), kind=kOutput, calls=%fused_computation.76 | convolution fusion | flops 1879506944 | bytes 9306112 | tf_op jit(solution)/shard_map/std,dp->stp/dot_general | solution.py:136
  38.8 3.8 %all-to-all-start = ((bf16[2,128,1792]{2,1,0:T(8,128)(2,1)}), bf16[2,128,1792]{2,1,0:T(8,128)(2,1)S(1)}, u32[]{:S(2)}, u32[]{:S(2)}) async-start(bf16[2,128,1792]{2,1,0:T(8,128)(2,1)} %fusion.37), calls=%async_computation | async-start | bytes 1835008 | tf_op jit(solution)/shard_map/all_to_all | solution.py:142
  42.6 4.7 %fusion.67 = (bf16[2,1,512,1024]{3,2,1,0:T(8,128)(2,1)}, bf16[2,1,512,1024]{3,2,1,0:T(8,128)(2,1)}) fusion(bf16[2,2,512,1024]{3,2,1,0:T(8,128)(2,1)} %bitcast.227), kind=kLoop, calls=%fused_computation.156 | loop fusion | bytes 8388608 | tf_op jit(solution)/shard_map/jit(dynamic_index_in_dim)/dynamic_slice | solution.py:265
  47.3 5.7 %all-to-all-done = bf16[2,128,1792]{2,1,0:T(8,128)(2,1)S(1)} async-done(((bf16[2,128,1792]{2,1,0:T(8,128)(2,1)}), bf16[2,128,1792]{2,1,0:T(8,128)(2,1)S(1)}, u32[]{:S(2)}, u32[]{:S(2)}) %all-to-all-start) | async-done | bytes 917536 | tf_op jit(solution)/shard_map/all_to_all | solution.py:142
  53.0 4.6 %all-to-all-start.1 = ((f32[2,2,128,256]{3,2,1,0:T(8,128)}), f32[2,2,128,256]{3,2,1,0:T(8,128)S(1)}, u32[]{:S(2)}, u32[]{:S(2)}) async-start(f32[2,2,128,256]{3,2,1,0:T(8,128)} %param.45), calls=%async_computation.1 | async-start | bytes 1048576 | tf_op jit(solution)/shard_map/all_to_all | solution.py:244
  57.7 0.9 fusion.69
  58.8 1.1 copy.83
  61.9 9.2 %while.46 = (s32[]{:T(128)}, f32[4,128,256]{2,1,0:T(8,128)S(1)}, f32[4,128]{1,0:T(4,128)S(1)}, f32[2,64,4,256]{3,1,0,2:T(8,128)}, f32[2,64,4,128]{3,2,1,0:T(4,12...) while((s32[]{:T(128)}, f32[4,128,256]{2,1,0:T(8,128)S(1)}, ...), condition=%wide.region_12.13_spmd.clone, body=%wide.region_10.12_spmd.clone.sunk | while | flops 279794688 | bytes 5934213 | solution.py:85
  61.9 0.9 constant_dynamic-slice_fusion.5
  63.9 1.2 fusion.109
  65.1 0.7 convolution_add_fusion.6
  65.8 0.7 fusion.110
  66.5 0.9 constant_dynamic-slice_fusion.5
  68.5 1.1 fusion.109
  69.6 0.7 convolution_add_fusion.6
  70.3 0.7 fusion.110
  71.2 12.0 %all_gather.25 = bf16[512,4,2,64]{0,3,2,1:T(8,128)(2,1)S(1)} all-gather(bf16[128,4,2,64]{0,3,2,1:T(8,128)(2,1)S(1)} %multiply_convert_fusion.3), channel_id=1, replica_groups=mesh['grp'=2,'sp'=4,'fs'=2,'tp'=2] {'sp'}, dimensions={0}, use_global_device_ids=true | all-gather | bytes 655360 | tf_op jit(solution)/shard_map/all_gather | solution.py:170
  83.2 1.1 copy.84
  84.3 2.0 %copy.101 = f32[128,4,256]{0,2,1:T(8,128)} copy(f32[128,4,256]{2,0,1:T(8,128)} %bitcast.255) | data formatting | bytes 1048576 | tf_op jit(solution)/shard_map/reshape | solution.py:98
  86.4 8.7 %all-gather.2 = f32[4,4,128]{2,1,0:T(4,128)S(1)} all-gather(f32[1,4,128]{2,1,0:T(4,128)S(1)} %bitcast.262), channel_id=2, replica_groups=mesh['grp'=2,'sp'=4,'fs'=2,'tp'=2] {'sp'}, dimensions={0}, use_global_device_ids=true | all-gather | bytes 10240 | tf_op jit(solution)/shard_map/all_gather | solution.py:18
  95.2 3.6 %collective-permute-start.1 = (bf16[128,4,128]{0,2,1:T(8,128)(2,1)}, bf16[128,4,128]{0,2,1:T(8,128)(2,1)S(1)}, u32[]{:S(2)}, u32[]{:S(2)}) collective-permute-start(bf16[128,4,128]{0,2,1:T(8,128)(2,1)} %collective-permute-done), channel_id=1, source_target_pairs={{0,4},{4,8},{8,12},{12,0},{1,5},{5,9},{9,13},{13,1},{2,6},{6,10},{... | collective-permute-start | bytes 393224 | tf_op jit(solution)/shard_map/ppermute | solution.py:173
  98.8 5.3 %collective-permute-done.1 = bf16[128,4,128]{0,2,1:T(8,128)(2,1)S(1)} collective-permute-done((bf16[128,4,128]{0,2,1:T(8,128)(2,1)}, bf16[128,4,128]{0,2,1:T(8,128)(2,1)S(1)}, u32[]{:S(2)}, u32[]{:S(2)}) %collective-permute-start.1) | collective-permute-done | bytes 131104 | tf_op jit(solution)/shard_map/ppermute | solution.py:173
  104.1 3.5 %collective-permute-start.2 = (bf16[128,4,128]{0,2,1:T(8,128)(2,1)S(1)}, bf16[128,4,128]{0,2,1:T(8,128)(2,1)S(1)}, u32[]{:S(2)}, u32[]{:S(2)}) collective-permute-start(bf16[128,4,128]{0,2,1:T(8,128)(2,1)S(1)} %collective-permute-done.1), channel_id=1, source_target_pairs={{0,4},{4,8},{8,12},{12,0},{1,5},{5,9},{9,13},{13,1},{2,6},{6,10},{... | collective-permute-start | bytes 393224 | tf_op jit(solution)/shard_map/ppermute | solution.py:173
  107.6 0.7 multiply_convert_fusion.2
  108.3 7.5 %collective-permute-done.2 = bf16[128,4,128]{0,2,1:T(8,128)(2,1)S(1)} collective-permute-done((bf16[128,4,128]{0,2,1:T(8,128)(2,1)S(1)}, bf16[128,4,128]{0,2,1:T(8,128)(2,1)S(1)}, u32[]{:S(2)}, u32[]{:S(2)}) %collective-permute-start.2) | collective-permute-done | bytes 131104 | tf_op jit(solution)/shard_map/ppermute | solution.py:173
  115.9 0.9 constant_dynamic-update-slice_fusion.6
  117.0 0.9 constant_dynamic-update-slice_fusion.2
  118.5 4.9 %while.47 = (s32[]{:T(128)}, f32[4,2,128]{2,1,0:T(2,128)S(1)}, f32[4,2,128]{2,1,0:T(2,128)S(1)}, f32[4,2,128,128]{3,2,1,0:T(8,128)S(1)}, s32[2]{0:T(128)S(1)}, /...) while((s32[]{:T(128)}, f32[4,2,128]{2,1,0:T(2,128)S(1)}, ...), condition=%wide.region_8.9_spmd.clone.clone, body=%wide.region_3.8_spmd.clone.clone.sunk | while | flops 102802176 | bytes 4989555 | solution.py:213
  118.5 0.6 dynamic_slice.117
  119.7 1.2 conditional.4
  120.9 0.6 dynamic_slice.117
  122.2 1.2 conditional.4
  123.9 10.8 %all_gather.26 = bf16[128,8,128]{2,0,1:T(8,128)(2,1)S(1)} all-gather(bf16[128,4,128]{2,0,1:T(8,128)(2,1)S(1)} %multiply_convert_fusion.1), channel_id=1, replica_groups=mesh['grp'=2,'sp'=4,'fs'=2,'tp'=2] {'tp'}, dimensions={1}, use_global_device_ids=true | all-gather | bytes 393216 | tf_op jit(solution)/shard_map/all_gather | solution.py:256
  134.7 0.8 copy.113
  135.5 0.8 copy.115
  136.3 2.0 %all-gather.8.cloned.1.call-done = f32[16,128,256]{2,1,0:T(8,128)} async-done(((f32[4,128,256]{2,1,0:T(8,128)}), f32[16,128,256]{2,1,0:T(8,128)}) %all-gather.8.cloned.1.call-update) | async-done | bytes 2097168 | tf_op jit(solution)/shard_map/all_gather | solution.py:18
  138.4 3.9 %while.45 = (s32[]{:T(128)}, f32[4,128]{1,0:T(4,128)S(1)}, f32[4,128,256]{2,1,0:T(8,128)S(1)}, s32[]{:T(128)}, f32[4,4,128]{2,1,0:T(4,128)S(1)}, /*index=5*/f32[...) while((s32[]{:T(128)}, f32[4,128]{1,0:T(4,128)S(1)}, f32[4,128,256]{2,1,0:T(8,128)S(1)}, s32[]{:T(128)}, ...), condition=%wide.region_14.15_spmd, body=%wide.region_13.14_spmd.sunk | while | flops 262661 | bytes 1583239 | solution.py:26
  138.4 1.3 bitcast_add_fusion.4
  139.8 1.2 bitcast_add_fusion.4
  141.0 1.2 bitcast_add_fusion.4
  142.4 2.3 %multiply_reduce_fusion = (f32[128,4]{0,1:T(4,128)S(1)}, f32[128,4,256]{0,2,1:T(8,128)S(1)}) fusion(f32[128,4,256]{0,2,1:T(8,128)} %copy.101, f32[4,128,256]{2,1,0:T(8,128)S(1)} %fusion.49, f32[128,4,128]{2,1,0:T(4,128)} %bitcast.259), kind=kOutput, calls=%fused_computation.104 | convolution fusion | flops 201719296 | bytes 1837056 | tf_op jit(solution)/shard_map/jwo,wos->jws/dot_general | solution.py:246
  144.8 0.8 multiply_convert_fusion
  145.6 1.1 copy.102
  146.7 2.3 %all_gather.31 = bf16[128,8,256]{2,0,1:T(8,128)(2,1)S(1)} all-gather(bf16[128,4,256]{2,0,1:T(8,128)(2,1)S(1)} %copy.102), channel_id=1, replica_groups=mesh['grp'=2,'sp'=4,'fs'=2,'tp'=2] {'tp'}, dimensions={1}, use_global_device_ids=true | all-gather | bytes 786432 | tf_op jit(solution)/shard_map/all_gather | solution.py:257
  149.0 0.7 fusion.70
  149.7 1.8 %copy.114 = bf16[128,4,256]{0,2,1:T(8,128)(2,1)} copy(bf16[128,4,256]{2,0,1:T(8,128)(2,1)} %get-tuple-element.513) | data formatting | bytes 524288
  151.5 0.8 copy.116
  152.4 2.2 %fusion.73 = f32[128,1024]{1,0:T(8,128)S(1)} fusion(bf16[128,1024]{0,1:T(8,128)(2,1)} %bitcast.252, bf16[1024,1024]{1,0:T(8,128)(2,1)} %bitcast.225), kind=kOutput, calls=%fused_computation.162 | convolution fusion | flops 268435456 | bytes 2883584 | tf_op jit(solution)/shard_map/dot_general | solution.py:277
  154.6 1.4 fusion.74
  156.0 1.6 convolution_add_fusion.3
  157.6 1.0 fusion.43
  (137 shorter events, 10.4 us)
Async XLA Ops:
  6.5 18.8 %copy-start = (bf16[2048,32]{0,1:T(8,128)(2,1)S(1)}, bf16[2048,32]{0,1:T(8,128)(2,1)}, u32[]{:S(2)}) copy-start(bf16[2048,32]{0,1:T(8,128)(2,1)} %param.36) | copy-start | bytes 393220
  6.5 8.2 %copy-start.1 = (f32[8]{0:T(128)S(1)}, f32[8]{0:T(128)}, u32[]{:S(2)}) copy-start(f32[8]{0:T(128)} %param.42) | copy-start | bytes 100
  6.5 8.8 %copy-start.11 = (f32[8,2,64]{2,1,0:T(2,128)S(1)}, f32[8,2,64]{2,1,0:T(2,128)}, u32[]{:S(2)}) copy-start(f32[8,2,64]{2,1,0:T(2,128)} %param.41) | copy-start | bytes 12292
  6.5 9.4 %copy-start.10 = (f32[8,128]{1,0:T(8,128)S(1)}, f32[8,128]{1,0:T(8,128)}, u32[]{:S(2)}) copy-start(f32[8,128]{1,0:T(8,128)} %param.38) | copy-start | bytes 12292
  6.5 10.0 %copy-start.2 = (f32[1,128,8]{1,2,0:T(8,128)S(1)}, f32[1,128,8]{1,2,0:T(8,128)}, u32[]{:S(2)}) copy-start(f32[1,128,8]{1,2,0:T(8,128)} %param.39) | copy-start | bytes 12292
  6.5 10.5 %copy-start.8 = (bf16[32,8,128]{2,1,0:T(8,128)(2,1)S(1)}, bf16[32,8,128]{2,1,0:T(8,128)(2,1)}, u32[]{:S(2)}) copy-start(bf16[32,8,128]{2,1,0:T(8,128)(2,1)} %param.37) | copy-start | bytes 196612
  6.6 25.8 %all-gather.6.cloned.1.call-start = ((), (), s32[]{:S(2)}) async-start(), calls=%async_computation.2 | async-start | bytes 1572864 | tf_op jit(solution)/shard_map/all_gather | solution.py:138
  10.0 15.4 %copy-start.7 = (bf16[1,128,2048]{2,1,0:T(8,128)(2,1)S(1)}, bf16[1,128,2048]{2,1,0:T(8,128)(2,1)}, u32[]{:S(2)}) copy-start(bf16[1,128,2048]{2,1,0:T(8,128)(2,1)} %fusion.48) | copy-start | bytes 1572868
  26.7 4.1 %copy-start.6 = (bf16[1024,1024]{1,0:T(8,128)(2,1)S(1)}, bf16[1024,1024]{1,0:T(8,128)(2,1)}, u32[]{:S(2)}) copy-start(bf16[1024,1024]{1,0:T(8,128)(2,1)} %param.46) | copy-start | bytes 6291460
  38.8 14.2 %all-to-all-start = ((bf16[2,128,1792]{2,1,0:T(8,128)(2,1)}), bf16[2,128,1792]{2,1,0:T(8,128)(2,1)S(1)}, u32[]{:S(2)}, u32[]{:S(2)}) async-start(bf16[2,128,1792]{2,1,0:T(8,128)(2,1)} %fusion.37), calls=%async_computation | async-start | bytes 1835008 | tf_op jit(solution)/shard_map/all_to_all | solution.py:142
  53.0 89.3 %all-to-all-start.1 = ((f32[2,2,128,256]{3,2,1,0:T(8,128)}), f32[2,2,128,256]{3,2,1,0:T(8,128)S(1)}, u32[]{:S(2)}, u32[]{:S(2)}) async-start(f32[2,2,128,256]{3,2,1,0:T(8,128)} %param.45), calls=%async_computation.1 | async-start | bytes 1048576 | tf_op jit(solution)/shard_map/all_to_all | solution.py:244
  57.7 80.6 %all-gather.8.cloned.1.call-start = ((), (), s32[]{:S(2)}) async-start(), calls=%async_computation.3 | async-start | bytes 2621440 | tf_op jit(solution)/shard_map/all_gather | solution.py:18
  58.8 36.4 %collective-permute-start = (bf16[128,4,128]{0,2,1:T(8,128)(2,1)S(1)}, bf16[128,4,128]{0,2,1:T(8,128)(2,1)}, u32[]{:S(2)}, u32[]{:S(2)}) collective-permute-start(bf16[128,4,128]{0,2,1:T(8,128)(2,1)S(1)} %bitcast.243), channel_id=1, source_target_pairs={{0,4},{4,8},{8,12},{12,0},{1,5},{5,9},{9,13},{13,1},{2,6},{6,10},{... | collective-permute-start | bytes 393224 | tf_op jit(solution)/shard_map/ppermute | solution.py:173
  71.0 13.3 %copy-start.3 = (f32[4,128,256]{2,1,0:T(8,128)}, f32[4,128,256]{2,1,0:T(8,128)S(1)}, u32[]{:S(2)}) copy-start(f32[4,128,256]{2,1,0:T(8,128)S(1)} %get-tuple-element.234) | copy-start | bytes 1572868
  95.2 8.9 %collective-permute-start.1 = (bf16[128,4,128]{0,2,1:T(8,128)(2,1)}, bf16[128,4,128]{0,2,1:T(8,128)(2,1)S(1)}, u32[]{:S(2)}, u32[]{:S(2)}) collective-permute-start(bf16[128,4,128]{0,2,1:T(8,128)(2,1)} %collective-permute-done), channel_id=1, source_target_pairs={{0,4},{4,8},{8,12},{12,0},{1,5},{5,9},{9,13},{13,1},{2,6},{6,10},{... | collective-permute-start | bytes 393224 | tf_op jit(solution)/shard_map/ppermute | solution.py:173
  104.1 11.8 %collective-permute-start.2 = (bf16[128,4,128]{0,2,1:T(8,128)(2,1)S(1)}, bf16[128,4,128]{0,2,1:T(8,128)(2,1)S(1)}, u32[]{:S(2)}, u32[]{:S(2)}) collective-permute-start(bf16[128,4,128]{0,2,1:T(8,128)(2,1)S(1)} %collective-permute-done.1), channel_id=1, source_target_pairs={{0,4},{4,8},{8,12},{12,0},{1,5},{5,9},{9,13},{13,1},{2,6},{6,10},{... | collective-permute-start | bytes 393224 | tf_op jit(solution)/shard_map/ppermute | solution.py:173
  118.4 5.3 %copy-start.13 = (f32[128]{0:T(128)S(1)}, f32[128]{0:T(128)}, u32[]{:S(2)}) copy-start(f32[128]{0:T(128)} %param.43) | copy-start | bytes 1540
  123.4 21.3 %copy-start.12 = (f32[256]{0:T(256)S(1)}, f32[256]{0:T(256)}, u32[]{:S(2)}) copy-start(f32[256]{0:T(256)} %param.44) | copy-start | bytes 3076
  138.3 16.2 %copy-start.4 = (bf16[2,1,512,1024]{3,2,1,0:T(8,128)(2,1)S(1)}, bf16[2,1,512,1024]{3,2,1,0:T(8,128)(2,1)}, u32[]{:S(2)}) copy-start(bf16[2,1,512,1024]{3,2,1,0:T(8,128)(2,1)} %get-tuple-element.506) | copy-start | bytes 6291460
  142.4 15.2 %copy-start.5 = (bf16[2,1,256,1024]{3,2,1,0:T(8,128)(2,1)S(1)}, bf16[2,1,256,1024]{3,2,1,0:T(8,128)(2,1)}, u32[]{:S(2)}) copy-start(bf16[2,1,256,1024]{3,2,1,0:T(8,128)(2,1)} %get-tuple-element.507) | copy-start | bytes 3145732
  152.4 5.3 %copy-start.9 = (bf16[128,4,128]{0,2,1:T(8,128)(2,1)S(1)}, bf16[128,4,128]{0,2,1:T(8,128)(2,1)}, u32[]{:S(2)}) copy-start(bf16[128,4,128]{0,2,1:T(8,128)(2,1)} %copy.115) | copy-start | bytes 393220
Sparse Core Ops, SparseCore 0:
  10.1 21.0 all-gather.5
  84.5 53.7 all-gather.7
